TPU v7x, 256 devices: a whole 4x4x8 slice. The times are simulated.
256 devices in a mesh: sp: 64 (over z, x, core), tp: 4 (over y).
Axes of the slice: x: 4, y: 4, z: 8, core: 2. Of those that a mesh axis runs over, the one named last changes fastest.
Arguments:
- queries: bfloat16 [32768, 2048], P('sp', 'tp'), may hold values from -90 to 90, as said below
- key_rows: bfloat16 [32768, 512], P('sp', 'tp'), may hold values from -6 to 6
- value_rows: bfloat16 [32768, 512], P('sp', 'tp'), may hold values from -6 to 6
- sink_logits: float32 [16], P('tp'), may hold values from 2 to 7
- residual: bfloat16 [32768, 2048], P('sp'), may hold values from -6 to 6
- norm_gain: float32 [2048], replicated, may hold values from 0.1 to 1.9
- out_weight: bfloat16 [2048, 2048], P('tp'), may hold values from -1.5 to 1.5
- gate_weight: bfloat16 [2048, 5632], P('sp', 'tp'), may hold values from -0.125 to 0.125
- up_weight: bfloat16 [2048, 5632], P('sp', 'tp'), may hold values from -0.125 to 0.125
- down_weight: bfloat16 [5632, 2048], P('tp', 'sp'), may hold values from -0.078125 to 0.078125
Outputs:
- mixed: bfloat16 [32768, 2048], P(('sp', 'tp'))
Inputs may be any that keep to these rules, and one draw needn't show every extreme that they name: queries are mostly of order one; some rows may be much larger.
All inputs are finite; a program needn't handle non-finite values.
Results may differ from a plain program's by a relative error of at most 0.012.
Values may be sent and summed in bfloat16 or wider, within the bound.
A program may use at most 128 MiB of HBM per device.

v0:
```python
import jax
import jax.numpy as jnp
from jax import lax
from jax.sharding import PartitionSpec as P

DH = 128
WIN = 128
EPSILON = 1e-06
MASKED = -1e30


def with_halo(cells, sides, width):
    for axis, dim in sides:
        count = lax.axis_size(axis)
        ends = count - 1
        head = lax.slice_in_dim(cells, 0, width, axis=dim)
        tail = lax.slice_in_dim(cells, cells.shape[dim] - width, cells.shape[dim], axis=dim)
        cells = jnp.concatenate(
            [
                lax.ppermute(tail, axis, [(i, (i + 1) % count) for i in range(ends)]),
                cells,
                lax.ppermute(head, axis, [((i + 1) % count, i) for i in range(ends)]),
            ],
            axis=dim,
        )
    return cells


def split_up(value, dim, size):
    before, after = (value.shape[:dim], value.shape[dim + 1 :])
    return jnp.moveaxis(value.reshape(*before, size, -1, *after), dim, 0)


def sent_and_summed(value, axis, dim):
    size = lax.axis_size(axis)
    blocks = lax.all_to_all(split_up(value, dim, size), axis, 0, 0, tiled=True)
    return jnp.sum(blocks.astype(jnp.float32), axis=0)


def sent_to_all(value, axis):
    size = lax.axis_size(axis)
    return lax.all_to_all(
        jnp.broadcast_to(value[None], (size, *value.shape)), axis, 0, 0, tiled=True
    )


def laid_out(blocks, dim):
    blocks = jnp.moveaxis(blocks, 0, dim)
    lengths = blocks.shape
    return blocks.reshape(*lengths[:dim], lengths[dim] * lengths[dim + 1], *lengths[dim + 2 :])


def gather_directly(value, axis, dim):
    blocks = sent_to_all(value, axis)
    return laid_out(blocks, dim)


def side_by_side(arrays, axis, dim, along):
    ends, at = ([], 0)
    for a in arrays[:-1]:
        at += a.shape[along]
        ends.append(at)
    both = jnp.concatenate(arrays, axis=along)
    return tuple(jnp.split(lax.all_gather(both, axis, axis=dim, tiled=True), ends, axis=along))


def attend_block(query_blk, key_blk, value_blk, sink_logits, query_pos, key_pos, seq_len):
    kv_heads = key_blk.shape[1] // DH
    group_size = query_blk.shape[1] // key_blk.shape[1]
    query_four = query_blk.reshape(query_blk.shape[0], kv_heads, group_size, DH)
    key_three = key_blk.reshape(key_blk.shape[0], kv_heads, DH)
    value_three = value_blk.reshape(value_blk.shape[0], kv_heads, DH)
    scores = jnp.einsum(
        "qhgd,khd->hgqk", query_four, key_three, preferred_element_type=jnp.float32
    ) * DH ** (-0.5)
    allowed = (
        (jnp.abs(key_pos[None, :] - query_pos[:, None]) <= WIN)
        & (key_pos[None, :] >= 0)
        & (key_pos[None, :] < seq_len)
    )
    scores = jnp.where(allowed[None, None], scores, MASKED)
    sink_col = sink_logits.reshape(kv_heads, group_size)[:, :, None]
    highest = jnp.maximum(jnp.max(scores, axis=-1), sink_col)
    weights_exp = jnp.exp(scores - highest[..., None])
    denominator = jnp.sum(weights_exp, axis=-1) + jnp.exp(sink_col - highest)
    probabilities = (weights_exp / denominator[..., None]).astype(jnp.bfloat16)
    heads_out = jnp.einsum(
        "hgqk,khd->qhgd", probabilities, value_three, preferred_element_type=jnp.float32
    )
    return heads_out.astype(jnp.bfloat16).reshape(query_blk.shape[0], kv_heads * group_size * DH)


def rms_scale(rows_wide, norm_gain):
    mean_square = jnp.mean(rows_wide * rows_wide, axis=-1, keepdims=True)
    return (rows_wide * lax.rsqrt(mean_square + EPSILON) * norm_gain).astype(jnp.bfloat16)


def fetch_down(down_weight):
    return lax.all_gather(down_weight, "sp", axis=1, tiled=True)


def shards(
    queries,
    key_rows,
    value_rows,
    sink_logits,
    residual,
    norm_gain,
    out_weight,
    gate_weight,
    up_weight,
    down_weight,
):
    tok_local = queries.shape[0]
    block_len = 2 * WIN
    share_rows = tok_local // lax.axis_size("tp")
    seq_len = tok_local * lax.axis_size("sp")
    device_offset = lax.axis_index("sp") * tok_local
    kv_pair = jnp.stack([key_rows, value_rows])
    kv_ext = with_halo(kv_pair, (("sp", 1),), WIN)

    def one_block(block_index):
        block_first = block_index * block_len
        query_blk = lax.dynamic_slice_in_dim(queries, block_first, block_len, 0)
        key_blk = lax.dynamic_slice_in_dim(kv_ext[0], block_first, block_len + 2 * WIN, 0)
        value_blk = lax.dynamic_slice_in_dim(kv_ext[1], block_first, block_len + 2 * WIN, 0)
        query_pos = device_offset + block_first + jnp.arange(block_len, dtype=jnp.int32)
        key_pos = (
            device_offset + block_first - WIN + jnp.arange(block_len + 2 * WIN, dtype=jnp.int32)
        )
        return attend_block(query_blk, key_blk, value_blk, sink_logits, query_pos, key_pos, seq_len)

    blocks = lax.map(one_block, jnp.arange(tok_local // block_len, dtype=jnp.int32))
    attended = blocks.reshape(tok_local, queries.shape[1])
    own_first = lax.axis_index("tp") * share_rows
    picked = attended
    attn_share = sent_and_summed(
        jnp.dot(picked, out_weight, preferred_element_type=jnp.float32).astype(jnp.bfloat16),
        "tp",
        0,
    )
    middle_own = (
        lax.dynamic_slice_in_dim(residual, own_first, share_rows, 0).astype(jnp.float32)
        + attn_share
    )
    normed_all = gather_directly(rms_scale(middle_own, norm_gain), "tp", 0)
    pieces = side_by_side((gate_weight, up_weight), "sp", 0, 1)
    gate_sectioned = pieces[0]
    up_sectioned = pieces[1]
    gate_acc = jnp.dot(normed_all, gate_sectioned, preferred_element_type=jnp.float32)
    up_acc = jnp.dot(normed_all, up_sectioned, preferred_element_type=jnp.float32)
    down_whole = fetch_down(down_weight)
    hidden = (jax.nn.silu(gate_acc) * up_acc).astype(jnp.bfloat16)
    picked = hidden
    ffn_share = lax.psum_scatter(
        jnp.dot(picked, down_whole, preferred_element_type=jnp.float32).astype(jnp.bfloat16),
        "tp",
        scatter_dimension=0,
        tiled=True,
    ).astype(jnp.float32)
    return (middle_own + ffn_share).astype(jnp.bfloat16)


def solution(mesh):
    placed = (
        P("sp", "tp"),
        P("sp", "tp"),
        P("sp", "tp"),
        P("tp"),
        P("sp", None),
        P(),
        P("tp", None),
        P("sp", "tp"),
        P("sp", "tp"),
        P("tp", "sp"),
    )
    return jax.shard_map(
        shards, mesh=mesh, in_specs=placed, out_specs=P(("sp", "tp"), None), check_vma=False
    )
```

profile of v0, /device:TPU:1, one launch (start us, length us, event | category | flops | bytes accessed | tf_op | source)
XLA Modules:
  0.0 233.1 jit_solution(577112236005821725)
XLA Ops:
  6.5 1.8 pad_maximum_fusion.1
  8.3 0.0 all-gather.5.cloned.1.call-start
  8.4 0.7 all-gather.5.cloned.1.call-update
  9.1 0.8 pad_maximum_fusion.3
  9.9 4.5 %collective-permute-start = (bf16[2,128,128]{2,1,0:T(8,128)(2,1)S(1)}, bf16[2,128,128]{2,1,0:T(8,128)(2,1)S(1)}, u32[]{:S(2)}, u32[]{:S(2)}) collective-permute-start(bf16[2,128,128]{2,1,0:T(8,128)(2,1)S(1)} %get-tuple-element.122), channel_id=1, source_target_pairs={{0,4},{4,8},{8,12},{12,16},{16,20},{20,24},{24,28},{28,32},{32,36}... | collective-permute-start | bytes 196616 | tf_op jit(solution)/shard_map/ppermute | solution.py:20
  14.4 1.9 collective-permute-start.1
  16.4 3.6 %collective-permute-done.1 = bf16[2,128,128]{2,1,0:T(8,128)(2,1)S(1)} collective-permute-done((bf16[2,128,128]{2,1,0:T(8,128)(2,1)S(1)}, bf16[2,128,128]{2,1,0:T(8,128)(2,1)S(1)}, u32[]{:S(2)}, u32[]{:S(2)}) %collective-permute-start.1) | collective-permute-done | bytes 65568 | tf_op jit(solution)/shard_map/ppermute | solution.py:22
  20.0 1.0 pad_maximum_fusion
  21.0 11.1 %while.12 = (s32[]{:T(128)}, bf16[2,256,512]{2,1,0:T(8,128)(2,1)}, bf16[2,768,128]{2,1,0:T(8,128)(2,1)S(1)}, s32[2]{0:T(128)S(1)}, s32[]{:T(128)}, /*index=5*/bf...) while((s32[]{:T(128)}, bf16[2,256,512]{2,1,0:T(8,128)(2,1)}, ...), condition=%wide.region_3.4_spmd, body=%wide.region_0.3_spmd.sunk | while | flops 273420544 | bytes 14467520 | solution.py:133
  21.0 0.6 dynamic_slice.48
  22.3 0.3 fusion.46
  22.6 1.0 constant_dynamic-slice_fusion.2
  23.6 0.1 copy.25
  23.7 0.5 fusion.47
  24.2 0.1 broadcast_maximum_fusion.2
  24.3 0.3 fusion.48
  24.6 0.1 exponential_add_fusion.2
  24.7 0.5 convolution_convert_fusion.4
  25.2 0.1 copy.26
  25.4 0.4 copy-done.4
  25.8 0.8 copy-done.5
  26.6 0.6 dynamic_slice.48
  27.8 0.3 fusion.46
  28.1 1.0 constant_dynamic-slice_fusion.2
  29.1 0.1 copy.25
  29.3 0.5 fusion.47
  29.8 0.1 broadcast_maximum_fusion.2
  29.8 0.3 fusion.48
  30.1 0.1 exponential_add_fusion.2
  30.2 0.5 convolution_convert_fusion.4
  30.8 0.1 copy.26
  30.9 0.4 copy-done.4
  31.3 0.8 copy-done.5
  32.1 3.6 %convolution_convert_fusion.1 = bf16[512,2048]{1,0:T(8,128)(2,1)} fusion(bf16[512,512]{1,0:T(8,128)(2,1)} %bitcast.59, bf16[512,2048]{1,0:T(8,128)(2,1)S(1)} %copy-done), kind=kOutput, calls=%fused_computation.30 | convolution fusion | flops 1074790400 | bytes 4718592 | tf_op jit(solution)/shard_map/dot_general | solution.py:138
  35.7 4.4 %all-to-all-start = ((bf16[4,128,2048]{2,1,0:T(8,128)(2,1)}), bf16[4,128,2048]{2,1,0:T(8,128)(2,1)}, u32[]{:S(2)}, u32[]{:S(2)}) async-start(bf16[4,128,2048]{2,1,0:T(8,128)(2,1)} %bitcast.52), calls=%async_computation | async-start | bytes 4194304 | tf_op jit(solution)/shard_map/all_to_all | solution.py:36
  40.2 0.0 reduce-scatter.2.cloned.1.call-start
  40.2 24.7 %all-to-all-done = bf16[4,128,2048]{2,1,0:T(8,128)(2,1)} async-done(((bf16[4,128,2048]{2,1,0:T(8,128)(2,1)}), bf16[4,128,2048]{2,1,0:T(8,128)(2,1)}, u32[]{:S(2)}, u32[]{:S(2)}) %all-to-all-start) | async-done | bytes 2097184 | tf_op jit(solution)/shard_map/all_to_all | solution.py:36
  64.9 2.2 convert_reduce_fusion
  67.2 0.2 multiply_reduce_fusion
  67.4 0.2 multiply_convert_fusion
  67.6 0.2 broadcast_in_dim.44
  67.9 30.0 %all_to_all.10 = bf16[4,128,2048]{2,1,0:T(8,128)(2,1)} all-to-all(bf16[4,128,2048]{2,1,0:T(8,128)(2,1)S(1)} %broadcast_in_dim.44), channel_id=1, replica_groups=mesh['sp'=64,'tp'=4] {'tp'}, dimensions={0} | all-to-all | bytes 4194304 | tf_op jit(solution)/shard_map/all_to_all | solution.py:42
  97.9 4.1 %all-gather.3.cloned.1.call-done = bf16[2048,2816]{1,0:T(8,128)(2,1)} async-done(((bf16[32,2816]{1,0:T(8,128)(2,1)}), bf16[2048,2816]{1,0:T(8,128)(2,1)}) %all-gather.3.cloned.1.call-update) | async-done | bytes 11534352 | tf_op jit(solution)/shard_map/all_gather | solution.py:64
  102.0 8.2 %fusion.14 = f32[512,1408]{1,0:T(8,128)} fusion(bf16[512,2048]{1,0:T(8,128)(2,1)} %bitcast.53, bf16[2048,2816]{1,0:T(8,128)(2,1)} %all-gather.3.cloned.1.call-done), kind=kOutput, calls=%fused_computation.25 | convolution fusion | flops 2952790016 | bytes 10747904 | tf_op jit(solution)/shard_map/dot_general | solution.py:150
  110.2 71.3 %all-gather.5.cloned.1.call-done = bf16[1408,2048]{0,1:T(8,128)(2,1)} async-done(((bf16[1408,32]{0,1:T(8,128)(2,1)}), bf16[1408,2048]{0,1:T(8,128)(2,1)}) %all-gather.5.cloned.1.call-update) | async-done | bytes 5767184 | tf_op jit(solution)/shard_map/all_gather | solution.py:99
  181.5 13.8 %convolution_convert_fusion.2 = bf16[512,2048]{1,0:T(8,128)(2,1)} fusion(bf16[1408,2048]{0,1:T(8,128)(2,1)} %all-gather.5.cloned.1.call-done, bf16[512,2048]{1,0:T(8,128)(2,1)} %bitcast.54, bf16[2048,2816]{1,0:T(8,128)(2,1)} %all-gather.3.cloned.1.call-done, f32[512,1408]{1,0:T(8,128)} %fusion.14), kind=kOutput, calls=%fused_computation.31 | convolution fusion | flops 5910953984 | bytes 18612224 | tf_op jit(solution)/shard_map/dot_general | solution.py:156
  195.4 29.0 %reduce-scatter.2.cloned.1.call-done = bf16[128,2048]{1,0:T(8,128)(2,1)} async-done(((bf16[512,2048]{1,0:T(8,128)(2,1)}), bf16[128,2048]{1,0:T(8,128)(2,1)}) %reduce-scatter.2.cloned.1.call-update) | async-done | bytes 524304 | tf_op jit(solution)/shard_map/reduce_scatter | solution.py:155
  224.4 2.2 add_convert_fusion
  (31 shorter events, 0.2 us)
Async XLA Ops:
  6.5 25.6 %copy-start = (bf16[512,2048]{1,0:T(8,128)(2,1)S(1)}, bf16[512,2048]{1,0:T(8,128)(2,1)}, u32[]{:S(2)}) copy-start(bf16[512,2048]{1,0:T(8,128)(2,1)} %param.18) | copy-start | bytes 6291460
  6.5 95.5 %all-gather.3.cloned.1.call-start = ((), (), s32[]{:S(2)}) async-start(), calls=%async_computation.3 | async-start | bytes 11714560 | tf_op jit(solution)/shard_map/all_gather | solution.py:64
  8.3 173.2 %all-gather.5.cloned.1.call-start = ((), (), s32[]{:S(2)}) async-start(), calls=%async_computation.4 | async-start | bytes 5857280 | tf_op jit(solution)/shard_map/all_gather | solution.py:99
  9.9 6.5 %collective-permute-start = (bf16[2,128,128]{2,1,0:T(8,128)(2,1)S(1)}, bf16[2,128,128]{2,1,0:T(8,128)(2,1)S(1)}, u32[]{:S(2)}, u32[]{:S(2)}) collective-permute-start(bf16[2,128,128]{2,1,0:T(8,128)(2,1)S(1)} %get-tuple-element.122), channel_id=1, source_target_pairs={{0,4},{4,8},{8,12},{12,16},{16,20},{20,24},{24,28},{28,32},{32,36}... | collective-permute-start | bytes 196616 | tf_op jit(solution)/shard_map/ppermute | solution.py:20
  14.4 5.6 %collective-permute-start.1 = (bf16[2,128,128]{2,1,0:T(8,128)(2,1)S(1)}, bf16[2,128,128]{2,1,0:T(8,128)(2,1)S(1)}, u32[]{:S(2)}, u32[]{:S(2)}) collective-permute-start(bf16[2,128,128]{2,1,0:T(8,128)(2,1)S(1)} %get-tuple-element.123), channel_id=1, source_target_pairs={{4,0},{8,4},{12,8},{16,12},{20,16},{24,20},{28,24},{32,28},{36,32}... | collective-permute-start | bytes 196616 | tf_op jit(solution)/shard_map/ppermute | solution.py:22
  23.6 0.7 copy-start.2
  24.7 1.0 copy-start.4
  25.8 0.8 copy-start.5
  29.1 0.7 copy-start.2
  30.2 1.0 copy-start.4
  31.3 0.8 copy-start.5
  35.7 29.2 %all-to-all-start = ((bf16[4,128,2048]{2,1,0:T(8,128)(2,1)}), bf16[4,128,2048]{2,1,0:T(8,128)(2,1)}, u32[]{:S(2)}, u32[]{:S(2)}) async-start(bf16[4,128,2048]{2,1,0:T(8,128)(2,1)} %bitcast.52), calls=%async_computation | async-start | bytes 4194304 | tf_op jit(solution)/shard_map/all_to_all | solution.py:36
  40.2 184.2 %reduce-scatter.2.cloned.1.call-start = ((), (), s32[]{:S(2)}) async-start(), calls=%async_computation.5 | async-start | bytes 2621440 | tf_op jit(solution)/shard_map/reduce_scatter | solution.py:155
  40.2 27.2 %copy-start.3 = (f32[2048]{0:T(1024)S(1)}, f32[2048]{0:T(1024)}, u32[]{:S(2)}) copy-start(f32[2048]{0:T(1024)} %param.17) | copy-start | bytes 24580
  64.9 2.2 copy-start.1
Sparse Core Ops, SparseCore 0:
  10.1 91.8 all-gather.2
  104.7 76.7 all-gather.4
  195.5 28.8 reduce-scatter.1
where the time goes:
time: 234 us; the launch traced here: 233 us
  waiting for transfers between devices  133 us (57%)
  blocking collectives  30 us (13%)
  matrix products  27.7 us (12%)
  between operations  13.2 us (6%)
  starting transfers between devices  10.9 us (5%)
  other arithmetic  9.91 us (4%)
  local copies, waits for them, and re-layouts  6.4 us (3%)
    all_gather x1, waiting for transfers between devices, fetch_down(): return lax.all_gather(down_weight, 'sp', axis=1, tiled=True)  71.3 us
    all_to_all x1, blocking collectives, sent_to_all(): lax.all_to_all(jnp.broadcast_to(value[None], (size, *value.shape)), axis,...  30 us
    reduce_scatter x1, waiting for transfers between devices, shards(): lax.psum_scatter(jnp.dot(picked, down_whole, preferred_element_type=jnp.f...  29 us
    all_to_all x1, waiting for transfers between devices, sent_and_summed(): blocks = lax.all_to_all(split_up(value, dim, size), axis, 0, 0, tiled=True)  24.7 us
    dot_general x1, matrix products, shards(): jnp.dot(picked, down_whole, preferred_element_type=jnp.float32)  13.8 us
    dot_general x1, matrix products, shards(): jnp.dot(normed_all, gate_sectioned, preferred_element_type=jnp.float32)  8.23 us
  transfers between devices with their start and end apart: 6, of which 5 were waited for; matrix products, arithmetic and copies ran while one was open for 10% of the time, Pallas kernels for 0%

commit v1 on v0

--- a/solution.py
+++ b/solution.py
@@ -7,6 +7,11 @@
 WIN = 128
 EPSILON = 1e-06
 MASKED = -1e30
+
+
+def all_parts(block, mesh_axis, along):
+    parts = lax.all_gather(block, mesh_axis)
+    return jnp.concatenate(parts, axis=along)
 
 
 def with_halo(cells, sides, width):
@@ -96,7 +101,7 @@
 
 
 def fetch_down(down_weight):
-    return lax.all_gather(down_weight, "sp", axis=1, tiled=True)
+    return all_parts(down_weight, "sp", 1)
 
 
 def shards(

time: 234 us -> 242 us (1.034)
  blocking collectives: 30 us -> 0 us
  waiting for transfers between devices: 133 us -> 157 us
  local copies, waits for them, and re-layouts: 6.4 us -> 17.1 us
  starting transfers between devices: 10.9 us -> 15.6 us
    all_gather x1, waiting for transfers between devices: 4.12 us -> 77.8 us  [side_by_side(): lax.all_gather(both, axis, axis=dim, tiled=True)]
    all_gather x1, waiting for transfers between devices: 71.3 us -> 20.9 us  [all_parts(): parts = lax.all_gather(block, mesh_axis)]
    all_to_all x1 -> x0, blocking collectives: 30 us -> none  [sent_to_all(): lax.all_to_all(jnp.broadcast_to(value[None], (size, *value.shape)), axis,...]
    reshape x0 -> x1, local copies, waits for them, and re-layouts: none -> 5.69 us  [all_parts(): return jnp.concatenate(parts, axis=along)]
    all_to_all x0 -> x1, starting transfers between devices: none -> 4.45 us  [sent_to_all(): lax.all_to_all(jnp.broadcast_to(value[None], (size, *value.shape)), axis,...]
    unnamed x6 -> x7, local copies, waits for them, and re-layouts: 0.02 us -> 3.63 us
  transfers between devices with their start and end apart: 6 -> 7, of which waited for: 5 -> 5; matrix products, arithmetic and copies ran while one was open for 10% -> 12% of each run, Pallas kernels for 0% -> 0%
where the time goes in v1:
time: 242 us; the launch traced here: 241 us
  waiting for transfers between devices  157 us (65%)
  matrix products  27.7 us (11%)
  local copies, waits for them, and re-layouts  17.1 us (7%)
  starting transfers between devices  15.6 us (6%)
  between operations  13.2 us (5%)
  other arithmetic  9.77 us (4%)
    all_gather x1, waiting for transfers between devices, side_by_side(): lax.all_gather(both, axis, axis=dim, tiled=True)  77.8 us
    reduce_scatter x1, waiting for transfers between devices, shards(): lax.psum_scatter(jnp.dot(picked, down_whole, preferred_element_type=jnp.f...  28.8 us
    all_to_all x1, waiting for transfers between devices, sent_and_summed(): blocks = lax.all_to_all(split_up(value, dim, size), axis, 0, 0, tiled=True)  24.7 us
    all_gather x1, waiting for transfers between devices, all_parts(): parts = lax.all_gather(block, mesh_axis)  20.9 us
    dot_general x1, matrix products, shards(): jnp.dot(picked, down_whole, preferred_element_type=jnp.float32)  13.8 us
    dot_general x1, matrix products, shards(): jnp.dot(normed_all, gate_sectioned, preferred_element_type=jnp.float32)  8.28 us
    reshape x1, local copies, waits for them, and re-layouts, all_parts(): return jnp.concatenate(parts, axis=along)  5.69 us
  transfers between devices with their start and end apart: 7, of which 5 were waited for; matrix products, arithmetic and copies ran while one was open for 12% of the time, Pallas kernels for 0%

profile of v1, /device:TPU:1, one launch (start us, length us, event | category | flops | bytes accessed | tf_op | source)
XLA Modules:
  0.0 241.4 jit_solution(190697894647127214)
XLA Ops:
  6.5 0.7 all-gather.6.cloned.1.call-update
  7.3 1.6 pad_maximum_fusion.1
  9.0 0.8 pad_maximum_fusion.3
  9.8 4.5 %collective-permute-start = (bf16[2,128,128]{2,1,0:T(8,128)(2,1)S(1)}, bf16[2,128,128]{2,1,0:T(8,128)(2,1)S(1)}, u32[]{:S(2)}, u32[]{:S(2)}) collective-permute-start(bf16[2,128,128]{2,1,0:T(8,128)(2,1)S(1)} %get-tuple-element.129), channel_id=1, source_target_pairs={{0,4},{4,8},{8,12},{12,16},{16,20},{20,24},{24,28},{28,32},{32,36}... | collective-permute-start | bytes 196616 | tf_op jit(solution)/shard_map/ppermute | solution.py:25
  14.3 1.9 collective-permute-start.1
  16.2 3.6 %collective-permute-done.1 = bf16[2,128,128]{2,1,0:T(8,128)(2,1)S(1)} collective-permute-done((bf16[2,128,128]{2,1,0:T(8,128)(2,1)S(1)}, bf16[2,128,128]{2,1,0:T(8,128)(2,1)S(1)}, u32[]{:S(2)}, u32[]{:S(2)}) %collective-permute-start.1) | collective-permute-done | bytes 65568 | tf_op jit(solution)/shard_map/ppermute | solution.py:27
  19.9 1.0 pad_maximum_fusion
  20.9 11.1 %while.12 = (s32[]{:T(128)}, bf16[2,256,512]{2,1,0:T(8,128)(2,1)}, bf16[2,768,128]{2,1,0:T(8,128)(2,1)S(1)}, s32[2]{0:T(128)S(1)}, s32[]{:T(128)}, /*index=5*/bf...) while((s32[]{:T(128)}, bf16[2,256,512]{2,1,0:T(8,128)(2,1)}, ...), condition=%wide.region_3.4_spmd, body=%wide.region_0.3_spmd.sunk | while | flops 273420544 | bytes 14467520 | solution.py:138
  20.9 0.6 dynamic_slice.48
  22.2 0.3 fusion.46
  22.5 1.0 constant_dynamic-slice_fusion.2
  23.5 0.1 copy.32
  23.6 0.5 fusion.47
  24.2 0.3 fusion.48
  24.5 0.1 exponential_add_fusion.2
  24.6 0.5 convolution_convert_fusion.4
  25.1 0.1 copy.33
  25.3 0.4 copy-done.4
  25.6 0.8 copy-done.5
  26.4 0.6 dynamic_slice.48
  27.7 0.3 fusion.46
  28.0 1.0 constant_dynamic-slice_fusion.2
  29.0 0.1 copy.32
  29.2 0.5 fusion.47
  29.7 0.1 broadcast_maximum_fusion.2
  29.7 0.3 fusion.48
  30.0 0.1 exponential_add_fusion.2
  30.1 0.5 convolution_convert_fusion.4
  30.6 0.1 copy.33
  30.8 0.4 copy-done.4
  31.2 0.8 copy-done.5
  32.0 3.6 %convolution_convert_fusion.1 = bf16[512,2048]{1,0:T(8,128)(2,1)} fusion(bf16[512,512]{1,0:T(8,128)(2,1)} %bitcast.67, bf16[512,2048]{1,0:T(8,128)(2,1)S(1)} %copy-done), kind=kOutput, calls=%fused_computation.30 | convolution fusion | flops 1074790400 | bytes 4718592 | tf_op jit(solution)/shard_map/dot_general | solution.py:143
  35.6 4.4 %all-to-all-start = ((bf16[4,128,2048]{2,1,0:T(8,128)(2,1)}), bf16[4,128,2048]{2,1,0:T(8,128)(2,1)}, u32[]{:S(2)}, u32[]{:S(2)}) async-start(bf16[4,128,2048]{2,1,0:T(8,128)(2,1)} %bitcast.62), calls=%async_computation | async-start | bytes 4194304 | tf_op jit(solution)/shard_map/all_to_all | solution.py:41
  40.1 24.7 %all-to-all-done = bf16[4,128,2048]{2,1,0:T(8,128)(2,1)} async-done(((bf16[4,128,2048]{2,1,0:T(8,128)(2,1)}), bf16[4,128,2048]{2,1,0:T(8,128)(2,1)}, u32[]{:S(2)}, u32[]{:S(2)}) %all-to-all-start) | async-done | bytes 2097184 | tf_op jit(solution)/shard_map/all_to_all | solution.py:41
  64.8 2.2 convert_reduce_fusion
  67.0 0.2 multiply_reduce_fusion
  67.3 0.2 multiply_convert_fusion
  67.5 1.6 broadcast_in_dim.44
  69.1 4.4 %all-to-all-start.1 = ((bf16[4,128,2048]{2,1,0:T(8,128)(2,1)}), bf16[4,128,2048]{2,1,0:T(8,128)(2,1)}, u32[]{:S(2)}, u32[]{:S(2)}) async-start(bf16[4,128,2048]{2,1,0:T(8,128)(2,1)} %broadcast_in_dim.44), calls=%async_computation.1 | async-start | bytes 4194304 | tf_op jit(solution)/shard_map/all_to_all | solution.py:47
  73.6 0.2 reduce-scatter.2.cloned.1.call-start
  73.8 20.9 %all-gather.6.cloned.1.call-done = bf16[90112,32]{0,1:T(8,128)(2,1)} async-done(((bf16[1408,32]{0,1:T(8,128)(2,1)}), bf16[90112,32]{0,1:T(8,128)(2,1)}) %all-gather.6.cloned.1.call-update) | async-done | bytes 5767184 | tf_op jit(solution)/shard_map/all_gather | solution.py:13
  94.7 3.6 %copy.29 = bf16[4,8,64,1408]{3,2,1,0:T(8,128)(2,1)S(1)} copy(bf16[4,8,64,1408]{3,1,2,0:T(8,128)(2,1)} %bitcast.60) | data formatting | bytes 11534336
  98.3 5.7 %copy.23 = bf16[1408,64,32]{0,2,1:T(8,128)(2,1)} copy(bf16[1408,64,32]{0,1,2:T(8,128)(2,1)S(1)} %bitcast.58) | data formatting | bytes 11534336 | tf_op jit(solution)/shard_map/reshape | solution.py:14
  104.0 77.8 %all-gather.4.cloned.1.call-done = bf16[2048,2816]{1,0:T(8,128)(2,1)} async-done(((bf16[32,2816]{1,0:T(8,128)(2,1)}), bf16[2048,2816]{1,0:T(8,128)(2,1)}) %all-gather.4.cloned.1.call-update) | async-done | bytes 11534352 | tf_op jit(solution)/shard_map/all_gather | solution.py:69
  181.8 8.3 %fusion.14 = f32[512,1408]{1,0:T(8,128)} fusion(bf16[512,2048]{1,0:T(8,128)(2,1)} %bitcast.16, bf16[2048,2816]{1,0:T(8,128)(2,1)} %all-gather.4.cloned.1.call-done), kind=kOutput, calls=%fused_computation.25 | convolution fusion | flops 2952790016 | bytes 10747904 | tf_op jit(solution)/shard_map/dot_general | solution.py:155
  190.1 13.8 %convolution_convert_fusion.2 = bf16[512,2048]{1,0:T(8,128)(2,1)} fusion(bf16[1408,2048]{0,1:T(8,128)(2,1)} %bitcast.61, bf16[512,2048]{1,0:T(8,128)(2,1)} %bitcast.16, bf16[2048,2816]{1,0:T(8,128)(2,1)} %all-gather.4.cloned.1.call-done, f32[512,1408]{1,0:T(8,128)} %fusion.14), kind=kOutput, calls=%fused_computation.31 | convolution fusion | flops 5910953984 | bytes 18612224 | tf_op jit(solution)/shard_map/dot_general | solution.py:161
  203.9 28.8 %reduce-scatter.2.cloned.1.call-done = bf16[128,2048]{1,0:T(8,128)(2,1)} async-done(((bf16[512,2048]{1,0:T(8,128)(2,1)}), bf16[128,2048]{1,0:T(8,128)(2,1)}) %reduce-scatter.2.cloned.1.call-update) | async-done | bytes 524304 | tf_op jit(solution)/shard_map/reduce_scatter | solution.py:160
  232.7 2.2 add_convert_fusion
  (34 shorter events, 0.3 us)
Async XLA Ops:
  6.5 25.4 %copy-start = (bf16[512,2048]{1,0:T(8,128)(2,1)S(1)}, bf16[512,2048]{1,0:T(8,128)(2,1)}, u32[]{:S(2)}) copy-start(bf16[512,2048]{1,0:T(8,128)(2,1)} %param.18) | copy-start | bytes 6291460
  6.5 88.1 %all-gather.6.cloned.1.call-start = ((), (), s32[]{:S(2)}) async-start(), calls=%async_computation.5 | async-start | bytes 5857280 | tf_op jit(solution)/shard_map/all_gather | solution.py:13
  7.3 174.6 %all-gather.4.cloned.1.call-start = ((), (), s32[]{:S(2)}) async-start(), calls=%async_computation.3 | async-start | bytes 11714560 | tf_op jit(solution)/shard_map/all_gather | solution.py:69
  9.8 6.5 %collective-permute-start = (bf16[2,128,128]{2,1,0:T(8,128)(2,1)S(1)}, bf16[2,128,128]{2,1,0:T(8,128)(2,1)S(1)}, u32[]{:S(2)}, u32[]{:S(2)}) collective-permute-start(bf16[2,128,128]{2,1,0:T(8,128)(2,1)S(1)} %get-tuple-element.129), channel_id=1, source_target_pairs={{0,4},{4,8},{8,12},{12,16},{16,20},{20,24},{24,28},{28,32},{32,36}... | collective-permute-start | bytes 196616 | tf_op jit(solution)/shard_map/ppermute | solution.py:25
  14.3 5.6 %collective-permute-start.1 = (bf16[2,128,128]{2,1,0:T(8,128)(2,1)S(1)}, bf16[2,128,128]{2,1,0:T(8,128)(2,1)S(1)}, u32[]{:S(2)}, u32[]{:S(2)}) collective-permute-start(bf16[2,128,128]{2,1,0:T(8,128)(2,1)S(1)} %get-tuple-element.130), channel_id=1, source_target_pairs={{4,0},{8,4},{12,8},{16,12},{20,16},{24,20},{28,24},{32,28},{36,32}... | collective-permute-start | bytes 196616 | tf_op jit(solution)/shard_map/ppermute | solution.py:27
  23.4 0.7 copy-start.2
  24.6 1.0 copy-start.4
  25.6 0.8 copy-start.5
  29.0 0.7 copy-start.2
  30.1 1.0 copy-start.4
  31.2 0.8 copy-start.5
  35.6 29.2 %all-to-all-start = ((bf16[4,128,2048]{2,1,0:T(8,128)(2,1)}), bf16[4,128,2048]{2,1,0:T(8,128)(2,1)}, u32[]{:S(2)}, u32[]{:S(2)}) async-start(bf16[4,128,2048]{2,1,0:T(8,128)(2,1)} %bitcast.62), calls=%async_computation | async-start | bytes 4194304 | tf_op jit(solution)/shard_map/all_to_all | solution.py:41
  40.1 27.2 %copy-start.3 = (f32[2048]{0:T(1024)S(1)}, f32[2048]{0:T(1024)}, u32[]{:S(2)}) copy-start(f32[2048]{0:T(1024)} %param.17) | copy-start | bytes 24580
  64.8 2.2 copy-start.1
  69.1 34.9 %all-to-all-start.1 = ((bf16[4,128,2048]{2,1,0:T(8,128)(2,1)}), bf16[4,128,2048]{2,1,0:T(8,128)(2,1)}, u32[]{:S(2)}, u32[]{:S(2)}) async-start(bf16[4,128,2048]{2,1,0:T(8,128)(2,1)} %broadcast_in_dim.44), calls=%async_computation.1 | async-start | bytes 4194304 | tf_op jit(solution)/shard_map/all_to_all | solution.py:47
  73.6 159.1 %reduce-scatter.2.cloned.1.call-start = ((), (), s32[]{:S(2)}) async-start(), calls=%async_computation.4 | async-start | bytes 2621440 | tf_op jit(solution)/shard_map/reduce_scatter | solution.py:160
Sparse Core Ops, SparseCore 0:
  10.0 84.5 all-gather.5
  97.4 84.3 all-gather.3
  204.0 28.5 reduce-scatter.1
